TPU v7x, 32 devices: a whole 2x2x4 slice. The times are simulated.
32 devices in a mesh: ep: 8 (over z, y), tp: 4 (over x, core).
Axes of the slice: x: 2, y: 2, z: 4, core: 2. Of those that a mesh axis runs over, the one named last changes fastest.
Arguments:
- tokens: bfloat16 [2048, 2048], P('ep'), may hold values from -6 to 6
- expert_ids: int32 [2048, 2], P('ep'), may hold values from 0 to 7, all different within a row; in each aligned block of 256 rows (0 to 255, 256 to 511, ...) at most 192 rows name the same one
- route_weight: float32 [2048, 2], P('ep'), may hold values from 0.1 to 1
- norm_gain: float32 [2048], replicated, may hold values from 0.1 to 1.9
- expert_gate: bfloat16 [8, 2048, 2048], P('ep', None, 'tp'), may hold values from -4 to 4
- expert_up: bfloat16 [8, 2048, 2048], P('ep', None, 'tp'), may hold values from -4 to 4
- expert_down: bfloat16 [8, 2048, 2048], P('ep', 'tp'), may hold values from -0.03125 to 0.03125
Outputs:
- combined: bfloat16 [2048, 2048], P('ep', 'tp')
Inputs may be any that keep to these rules, and one draw needn't show every extreme that they name: `expert_ids`: each row names 2 different experts. In each aligned block of 256 rows (the rows of one index of ep) no expert is named by more than 192 rows, and in some block one expert is named by exactly 192 rows.
All inputs are finite; a program needn't handle non-finite values.
Results may differ from a plain program's by a relative error of at most 0.012.
Values may be sent and summed in bfloat16 or wider, within the bound.
A program may use at most 128 MiB of HBM per device.

v0:
```python
import functools

import jax
import jax.numpy as jnp
from jax import lax
from jax.experimental import pallas as pl
from jax.experimental.pallas import tpu as pltpu
from jax.sharding import PartitionSpec as P

NORM_EPS = 1e-06
CLAMP_LIMIT = 7.0
SWISH_SCALE = 1.702
MESH = pl.DeviceIdType.MESH


def activate(gate_sum, up_sum):
    gate_cut = jnp.minimum(gate_sum, CLAMP_LIMIT)
    up_cut = jnp.clip(up_sum, -CLAMP_LIMIT, CLAMP_LIMIT)
    return ((up_cut + 1.0) * gate_cut * jax.nn.sigmoid(SWISH_SCALE * gate_cut)).astype(jnp.bfloat16)


def expert_kernel(
    groups,
    tokens,
    ids,
    route,
    gain,
    gate_hbm,
    up_hbm,
    down_hbm,
    out,
    gate_w,
    up_w,
    down_w,
    normed_own,
    normed_cross,
    before,
    send,
    send_cross,
    back,
    high,
    low,
    total_out,
    rows,
    part,
    pair_in,
    cross_out,
    cross_in,
    result,
    w_sem,
    disp_send,
    disp_recv,
    cross_send,
    cross_recv,
    core_send,
    core_recv,
    fwd_send,
    fwd_recv,
    pair_send,
    pair_recv,
    sum_send,
    sum_recv,
    ret_send,
    ret_recv,
):
    me = lax.axis_index("ep")
    tp = lax.axis_index("tp")
    a, b = tp // 2, lax.rem(tp, 2)
    cross = 2 * (1 - a) + b
    core = 2 * a + 1 - b
    capacity, quarter = send.shape[1:]
    tok_count = tokens.shape[0]
    half = groups // 2

    weights = [
        pltpu.make_async_copy(src, dst, w_sem.at[i])
        for i, (src, dst) in enumerate(((gate_hbm, gate_w), (up_hbm, up_w), (down_hbm, down_w)))
    ]

    def remote(src, dst, send_sem, recv_sem, ep_index, tp_index):
        return pltpu.make_async_remote_copy(
            src_ref=src,
            dst_ref=dst,
            send_sem=send_sem,
            recv_sem=recv_sem,
            device_id=(ep_index, tp_index),
            device_id_type=MESH,
        )

    def partner(k):
        total, bit = 0, 1
        while bit < groups:
            total += bit * lax.rem(me // bit + k // bit, 2)
            bit *= 2
        return total

    def order(i):
        i = i + (i // (groups - 2)) * (1 - 2 * lax.rem(i, 2))
        return i // 2 + half * lax.rem(i, 2)

    def dispatch(k):
        dst = partner(k)
        return remote(send.at[k], rows.at[k, tp], disp_send.at[k], disp_recv.at[k], dst, tp)

    def dispatch_cross(k):
        dst = partner(k)
        return remote(
            send_cross.at[k],
            rows.at[k, cross],
            cross_send.at[k],
            cross_recv.at[k],
            dst,
            tp,
        )

    def to_cross(k):
        return remote(rows.at[k, tp], rows.at[k, tp], cross_send.at[k], cross_recv.at[k], me, cross)

    def to_core(k):
        return remote(rows.at[k, tp], rows.at[k, tp], core_send.at[k], core_recv.at[k], me, core)

    def forward(k):
        return remote(rows.at[k, cross], rows.at[k, cross], fwd_send.at[k], fwd_recv.at[k], me, core)

    def pair(k):
        return remote(part.at[k, 1 - b], pair_in.at[k], pair_send.at[k], pair_recv.at[k], me, core)

    def cross_sum(k):
        return remote(cross_out.at[k], cross_in.at[k], sum_send.at[k], sum_recv.at[k], me, cross)

    def give_back(k):
        return remote(result.at[k], back.at[k], ret_send.at[k], ret_recv.at[k], partner(k), tp)

    for copy in weights:
        copy.start()

    barrier = pltpu.get_barrier_semaphore()

    def greet(k, carry):
        pl.semaphore_signal(
            barrier, inc=1, device_id=(lax.rem(me + k, groups), tp), device_id_type=MESH
        )
        return carry

    lax.fori_loop(1, groups, greet, 0)
    pl.semaphore_signal(barrier, inc=1, device_id=(me, cross), device_id_type=MESH)
    pl.semaphore_signal(barrier, inc=1, device_id=(me, core), device_id_type=MESH)

    values = tokens[...].astype(jnp.float32)
    scale = lax.rsqrt(jnp.mean(values * values, axis=-1, keepdims=True) + NORM_EPS)

    def normed(index):
        span = pl.ds(pl.multiple_of(index * quarter, quarter), quarter)
        return (tokens[:, span].astype(jnp.float32) * scale * gain[:, span]).astype(jnp.bfloat16)

    normed_own[...] = normed(tp)
    normed_cross[...] = normed(cross)
    earlier = lax.broadcasted_iota(jnp.int32, (tok_count, tok_count), 0)
    later = lax.broadcasted_iota(jnp.int32, (tok_count, tok_count), 1)
    before[...] = jnp.where(earlier < later, 1.0, 0.0).astype(jnp.bfloat16)

    def select(k):
        expert = partner(k)
        hits = ids[...] == expert
        named = jnp.sum(jnp.where(hits, 1.0, 0.0), axis=0, keepdims=True)
        weight = jnp.sum(jnp.where(hits, route[...], 0.0), axis=0, keepdims=True)
        count = jnp.dot(
            jnp.broadcast_to(named, (8, tok_count)).astype(jnp.bfloat16),
            before[...],
            preferred_element_type=jnp.float32,
        )[0:1]
        slot = jnp.where(named > 0.0, count.astype(jnp.int32), -1)
        place = lax.broadcasted_iota(jnp.int32, (capacity, tok_count), 0)
        chosen = place == slot
        mix = jnp.where(chosen, weight, 0.0)
        mix_high = mix.astype(jnp.bfloat16)
        high[k] = mix_high
        low[k] = (mix - mix_high.astype(jnp.float32)).astype(jnp.bfloat16)
        return jnp.where(chosen, 1.0, 0.0).astype(jnp.bfloat16)

    def pick(chosen, source):
        return jnp.dot(chosen, source[...], preferred_element_type=jnp.float32).astype(jnp.bfloat16)

    chosen = select(0)
    rows[0, tp] = pick(chosen, normed_own)
    rows[0, cross] = pick(chosen, normed_cross)
    pl.semaphore_wait(barrier, groups + 1)

    def launch(i, carry):
        k = order(i)
        chosen = select(k)
        send[k] = pick(chosen, normed_own)
        dispatch(k).start()

        @pl.when(k < half)
        def _():
            send_cross[k] = pick(chosen, normed_cross)
            dispatch_cross(k).start()

        return carry

    lax.fori_loop(1, groups, launch, 0)
    for copy in weights:
        copy.wait()

    def step(i, carry):
        @pl.when(i >= 4)
        def _():
            k = order(i - 4)
            cross_sum(k).wait_recv()
            total = part[k, b, a].astype(jnp.float32) + pair_in[k, a].astype(jnp.float32)
            total = (total + cross_in[k].astype(jnp.float32)).astype(jnp.bfloat16)

            @pl.when(k == 0)
            def _():
                back[0] = total

            @pl.when(k > 0)
            def _():
                result[k] = total
                give_back(k).start()

        @pl.when((i >= 3) & (i < groups + 3))
        def _():
            k = order(i - 3)
            pair(k).wait_recv()
            total = part[k, b, 1 - a].astype(jnp.float32) + pair_in[k, 1 - a].astype(jnp.float32)
            cross_out[k] = total.astype(jnp.bfloat16)
            cross_sum(k).start()

        @pl.when((i >= 2) & (i < groups + 2))
        def _():
            k = order(i - 2)
            to_core(k).wait_recv()
            forward(k).wait_recv()
            block = jnp.concatenate([rows[k, j] for j in range(4)], axis=1)
            gate_sum = jnp.dot(block, gate_w[...], preferred_element_type=jnp.float32)
            up_sum = jnp.dot(block, up_w[...], preferred_element_type=jnp.float32)
            activated = activate(gate_sum, up_sum)
            for j in range(4):
                part[k, j % 2, j // 2] = jnp.dot(
                    activated,
                    down_w[:, j * quarter : (j + 1) * quarter],
                    preferred_element_type=jnp.float32,
                ).astype(jnp.bfloat16)
            pair(k).start()

        @pl.when((i >= 1) & (i < groups + 1))
        def _():
            k = order(i - 1)

            @pl.when(k > 0)
            def _():
                to_cross(k).wait_recv()

            forward(k).start()

        @pl.when(i < groups)
        def _():
            k = order(i)

            @pl.when(k > 0)
            def _():
                dispatch(k).wait_recv()

            @pl.when(k >= half)
            def _():
                to_cross(k).start()

            to_core(k).start()

        return carry

    lax.fori_loop(0, groups + 4, step, 0)

    total_out[...] = jnp.zeros_like(total_out)

    def finish(i, carry):
        k = order(i)

        @pl.when(k > 0)
        def _():
            give_back(k).wait_recv()

        for share in (high, low):
            total_out[...] += lax.dot_general(
                share[k], back[k], (((0,), (0,)), ((), ())), preferred_element_type=jnp.float32
            )
        return carry

    lax.fori_loop(0, groups, finish, 0)
    out[...] = total_out[...].astype(jnp.bfloat16)

    def drain(k, carry):
        to_core(k).wait_send()
        forward(k).wait_send()
        pair(k).wait_send()
        cross_sum(k).wait_send()

        @pl.when(k > 0)
        def _():
            to_cross(k).wait_send()
            dispatch(k).wait_send()
            give_back(k).wait_send()

        return carry

    lax.fori_loop(0, groups, drain, 0)


def shards(tokens, expert_ids, route_weight, norm_gain, expert_gate, expert_up, expert_down):
    groups = lax.axis_size("ep")
    tp_count = lax.axis_size("tp")
    experts = groups * expert_gate.shape[0]
    tok_count, model_width = tokens.shape
    top_count = expert_ids.shape[1]
    capacity = min(tok_count, 3 * tok_count * top_count // experts)
    quarter = model_width // tp_count
    bf16 = jnp.bfloat16
    slots = (groups, capacity, quarter)
    weights = (expert_gate[0], expert_up[0], expert_down[0])
    return pl.pallas_call(
        functools.partial(expert_kernel, groups),
        out_shape=jax.ShapeDtypeStruct((tok_count, quarter), bf16),
        in_specs=[pl.BlockSpec(memory_space=pltpu.VMEM)] * 4
        + [pl.BlockSpec(memory_space=pl.ANY)] * 3,
        out_specs=pl.BlockSpec(memory_space=pltpu.VMEM),
        scratch_shapes=[
            *[pltpu.VMEM(weight.shape, bf16) for weight in weights],
            pltpu.VMEM((tok_count, quarter), bf16),
            pltpu.VMEM((tok_count, quarter), bf16),
            pltpu.VMEM((tok_count, tok_count), bf16),
            pltpu.VMEM(slots, bf16),
            pltpu.VMEM((groups // 2, capacity, quarter), bf16),
            pltpu.VMEM(slots, bf16),
            pltpu.VMEM((groups, capacity, tok_count), bf16),
            pltpu.VMEM((groups, capacity, tok_count), bf16),
            pltpu.VMEM((tok_count, quarter), jnp.float32),
            pltpu.VMEM((groups, 4, capacity, quarter), bf16),
            pltpu.VMEM((groups, 2, 2, capacity, quarter), bf16),
            pltpu.VMEM((groups, 2, capacity, quarter), bf16),
            pltpu.VMEM(slots, bf16),
            pltpu.VMEM(slots, bf16),
            pltpu.VMEM(slots, bf16),
            pltpu.SemaphoreType.DMA((3,)),
            *[pltpu.SemaphoreType.DMA((groups,)) for _ in range(14)],
        ],
        compiler_params=pltpu.CompilerParams(
            collective_id=0, has_side_effects=True, vmem_limit_bytes=60 * 1024 * 1024
        ),
    )(tokens, expert_ids.T, route_weight.T, norm_gain[None, :], *weights)


def solution(mesh):
    return jax.shard_map(
        shards,
        mesh=mesh,
        in_specs=(
            P("ep", None),
            P("ep", None),
            P("ep", None),
            P(),
            P("ep", None, "tp"),
            P("ep", None, "tp"),
            P("ep", "tp", None),
        ),
        out_specs=P("ep", "tp"),
        check_vma=False,
    )
```

profile of v0, /device:TPU:0, one launch (start us, length us, event | category | flops | bytes accessed | tf_op | source)
XLA Modules:
  0.0 87.7 jit_solution(11846666981663500931)
XLA Ops:
  0.0 86.0 %shard_map.73 = bf16[256,512]{1,0:T(8,128)(2,1)} custom-call(bf16[256,2048]{1,0:T(8,128)(2,1)} %tokens.1, s32[2,256]{1,0:T(2,128)} %bitcast.10, f32[2,256]{1,0:T(2,128)} %bitcast.11, f32[1,2048]{1,0:T(1,128)} %bitcast.9, bf16[2048,512]{1,0:T(8,128)(2,1)} %bitcast.6, bf16[2048,512]{1,0:T(8,128)(2,1)} %bitcast.7, bf16[512,2048]{1,0:T(8,128)(2,1)} %bitcast.8), custom_call_target="tpu_custom_call" | custom-call | tf_op jit(solution)/shard_map/pallas_call | solution.py:322
  86.0 1.7 %copy.9 = bf16[256,512]{1,0:T(8,128)(2,1)} copy(bf16[256,512]{1,0:T(8,128)(2,1)} %shard_map.73) | data formatting | bytes 524288
where the time goes:
time: 87.9 us; the launch traced here: 87.7 us
  Pallas kernels  86 us (98%)
  local copies, waits for them, and re-layouts  1.67 us (2%)
    pallas_call x1, Pallas kernels, shards(): pl.pallas_call(functools.partial(expert_kernel, groups), out_shape=jax.Sh...  86 us

commit v1 on v0

--- a/solution.py
+++ b/solution.py
@@ -11,6 +11,7 @@
 CLAMP_LIMIT = 7.0
 SWISH_SCALE = 1.702
 MESH = pl.DeviceIdType.MESH
+VISITS = (0, 2, 7, 6, 1, 4, 3, 5)
 
 
 def activate(gate_sum, up_sum):
@@ -95,8 +96,9 @@
         return total
 
     def order(i):
-        i = i + (i // (groups - 2)) * (1 - 2 * lax.rem(i, 2))
-        return i // 2 + half * lax.rem(i, 2)
+        turn = lax.rem(i, len(VISITS))
+        first = sum(place * (turn == n).astype(jnp.int32) for n, place in enumerate(VISITS))
+        return first * (groups // len(VISITS)) + i // len(VISITS)
 
     def dispatch(k):
         dst = partner(k)
@@ -204,22 +206,6 @@
         copy.wait()
 
     def step(i, carry):
-        @pl.when(i >= 4)
-        def _():
-            k = order(i - 4)
-            cross_sum(k).wait_recv()
-            total = part[k, b, a].astype(jnp.float32) + pair_in[k, a].astype(jnp.float32)
-            total = (total + cross_in[k].astype(jnp.float32)).astype(jnp.bfloat16)
-
-            @pl.when(k == 0)
-            def _():
-                back[0] = total
-
-            @pl.when(k > 0)
-            def _():
-                result[k] = total
-                give_back(k).start()
-
         @pl.when((i >= 3) & (i < groups + 3))
         def _():
             k = order(i - 3)
@@ -245,6 +231,36 @@
                 ).astype(jnp.bfloat16)
             pair(k).start()
 
+        @pl.when(i >= 4)
+        def _():
+            k = order(i - 4)
+            cross_sum(k).wait_recv()
+            total = part[k, b, a].astype(jnp.float32) + pair_in[k, a].astype(jnp.float32)
+            total = (total + cross_in[k].astype(jnp.float32)).astype(jnp.bfloat16)
+
+            @pl.when(k == 0)
+            def _():
+                back[0] = total
+
+            @pl.when(k > 0)
+            def _():
+                result[k] = total
+                give_back(k).start()
+
+        @pl.when(i < groups)
+        def _():
+            k = order(i)
+
+            @pl.when(k > 0)
+            def _():
+                dispatch(k).wait_recv()
+
+            @pl.when(k >= half)
+            def _():
+                to_cross(k).start()
+
+            to_core(k).start()
+
         @pl.when((i >= 1) & (i < groups + 1))
         def _():
             k = order(i - 1)
@@ -254,20 +270,6 @@
                 to_cross(k).wait_recv()
 
             forward(k).start()
-
-        @pl.when(i < groups)
-        def _():
-            k = order(i)
-
-            @pl.when(k > 0)
-            def _():
-                dispatch(k).wait_recv()
-
-            @pl.when(k >= half)
-            def _():
-                to_cross(k).start()
-
-            to_core(k).start()
 
         return carry
 

time: 87.9 us -> 87 us (0.990)
  no operation moved by 1% of the time
where the time goes in v1:
time: 87 us; the launch traced here: 86.8 us
  Pallas kernels  85.2 us (98%)
  local copies, waits for them, and re-layouts  1.67 us (2%)
    pallas_call x1, Pallas kernels, shards(): pl.pallas_call(functools.partial(expert_kernel, groups), out_shape=jax.Sh...  85.2 us

profile of v1, /device:TPU:0, one launch (start us, length us, event | category | flops | bytes accessed | tf_op | source)
XLA Modules:
  0.0 86.8 jit_solution(15549898600425126642)
XLA Ops:
  0.0 85.2 %shard_map.73 = bf16[256,512]{1,0:T(8,128)(2,1)} custom-call(bf16[256,2048]{1,0:T(8,128)(2,1)} %tokens.1, s32[2,256]{1,0:T(2,128)} %bitcast.10, f32[2,256]{1,0:T(2,128)} %bitcast.11, f32[1,2048]{1,0:T(1,128)} %bitcast.9, bf16[2048,512]{1,0:T(8,128)(2,1)} %bitcast.6, bf16[2048,512]{1,0:T(8,128)(2,1)} %bitcast.7, bf16[512,2048]{1,0:T(8,128)(2,1)} %bitcast.8), custom_call_target="tpu_custom_call" | custom-call | tf_op jit(solution)/shard_map/pallas_call | solution.py:324
  85.2 1.7 %copy.9 = bf16[256,512]{1,0:T(8,128)(2,1)} copy(bf16[256,512]{1,0:T(8,128)(2,1)} %shard_map.73) | data formatting | bytes 524288

commit v2 on v0

--- a/solution.py
+++ b/solution.py
@@ -11,12 +11,392 @@
 CLAMP_LIMIT = 7.0
 SWISH_SCALE = 1.702
 MESH = pl.DeviceIdType.MESH
+STEPS = (
+    "L30", "M0", "Y00", "A00", "L31", "F00", "G000", "G001", "L20", "M3",
+    "Y30", "A30", "L11", "B01", "L21", "H001", "B00", "B30", "A31", "F01",
+    "Y31", "G010", "X300", "M2", "A20", "Y20", "X301", "L10", "B31", "F30",
+    "B20", "Y21", "A21", "X310", "M1", "A11", "X311", "Y11", "G300", "F31",
+    "B21", "X210", "X200", "G311", "G310", "G301", "A10", "H300", "Y10", "X201",
+    "G011", "H000", "X211", "F10", "H311", "F20", "F21", "G100", "H301", "B11",
+    "H310", "B10", "G210", "S31", "G200", "F11", "H010", "S30", "G110", "G211",
+    "G111", "H210", "H200", "G201", "H011", "H100", "G101", "H110", "S20", "H211",
+    "J30", "H111", "S00", "S10", "H201", "H101", "S21", "J31", "J10", "S11",
+    "S01", "J20", "J11", "J21",
+)
+PLANES = 1 + max(int(step[1]) for step in STEPS)
+PARTS = 2
 
 
 def activate(gate_sum, up_sum):
     gate_cut = jnp.minimum(gate_sum, CLAMP_LIMIT)
     up_cut = jnp.clip(up_sum, -CLAMP_LIMIT, CLAMP_LIMIT)
     return ((up_cut + 1.0) * gate_cut * jax.nn.sigmoid(SWISH_SCALE * gate_cut)).astype(jnp.bfloat16)
+
+
+def plane_kernel(
+    groups,
+    tokens,
+    ids,
+    route,
+    gain,
+    gate_hbm,
+    up_hbm,
+    down_hbm,
+    out,
+    gate_w,
+    up_w,
+    down_w,
+    before,
+    meta,
+    normed,
+    dense,
+    picker,
+    high,
+    low,
+    rows,
+    picked,
+    part,
+    pair_in,
+    cross_out,
+    cross_in,
+    result,
+    plane_in,
+    total,
+    sum_out,
+    sum_in,
+    w_sem,
+    meta_send,
+    meta_recv,
+    dense_send,
+    dense_recv,
+    pick_send,
+    pick_recv,
+    core_send,
+    core_recv,
+    fwd_send,
+    fwd_recv,
+    pair_send,
+    pair_recv,
+    cross_send,
+    cross_recv,
+    near_send,
+    near_recv,
+    sum_send,
+    sum_recv,
+):
+    me = lax.axis_index("ep")
+    tp = lax.axis_index("tp")
+    a, b = tp // 2, lax.rem(tp, 2)
+    cross = 2 * (1 - a) + b
+    core = 2 * a + 1 - b
+    quarters = (tp, cross)
+    slots, width = rows.shape[3:]
+    quarter = PARTS * width
+    tok_count = tokens.shape[0]
+    f32, bf16 = jnp.float32, jnp.bfloat16
+
+    def partner(k):
+        total, bit = 0, 1
+        while bit < groups:
+            total += bit * lax.rem(me // bit + k // bit, 2)
+            bit *= 2
+        return total
+
+    def remote(src, dst, send_sem, recv_sem, k, tp_index):
+        return pltpu.make_async_remote_copy(
+            src_ref=src,
+            dst_ref=dst,
+            send_sem=send_sem,
+            recv_sem=recv_sem,
+            device_id=(partner(k), tp_index),
+            device_id_type=MESH,
+        )
+
+    def shares(d):
+        return range(2 if d < PLANES // 2 else 1)
+
+    def describe(d):
+        return remote(meta.at[0], meta.at[d], meta_send.at[d], meta_recv.at[d], 2 * d, tp)
+
+    def spread(d, q, h):
+        return remote(
+            normed.at[quarters[q], h],
+            dense.at[d - 1, q, h],
+            dense_send.at[d, q, h],
+            dense_recv.at[d, q, h],
+            2 * d,
+            tp,
+        )
+
+    def neighbour(d, q, h):
+        return remote(
+            picked.at[d, q, h],
+            rows.at[2 * d + 1, quarters[q], h],
+            pick_send.at[d, q, h],
+            pick_recv.at[d, q, h],
+            1,
+            tp,
+        )
+
+    def to_core(k, q, h):
+        ref = rows.at[k, quarters[q], h]
+        return remote(ref, ref, core_send.at[k, q, h], core_recv.at[k, q, h], 0, core)
+
+    def to_cross(k, h):
+        ref = rows.at[k, tp, h]
+        return remote(ref, ref, fwd_send.at[k, h], fwd_recv.at[k, h], 0, cross)
+
+    def pair(k, h):
+        return remote(
+            part.at[k, 1 - b, h], pair_in.at[k, h], pair_send.at[k, h], pair_recv.at[k, h], 0, core
+        )
+
+    def cross_sum(k, h):
+        return remote(
+            cross_out.at[k, h], cross_in.at[k, h], cross_send.at[k, h], cross_recv.at[k, h], 0, cross
+        )
+
+    def near_sum(d, h):
+        return remote(
+            result.at[2 * d + 1, h], plane_in.at[d, h], near_send.at[d, h], near_recv.at[d, h], 1, tp
+        )
+
+    def plane_sum(d, h):
+        return remote(
+            sum_out.at[d - 1, h], sum_in.at[d - 1, h], sum_send.at[d, h], sum_recv.at[d, h], 2 * d, tp
+        )
+
+    weights = [
+        pltpu.make_async_copy(src, dst, w_sem.at[i])
+        for i, (src, dst) in enumerate(((gate_hbm, gate_w), (up_hbm, up_w), (down_hbm, down_w)))
+    ]
+    for copy in weights:
+        copy.start()
+
+    barrier = pltpu.get_barrier_semaphore()
+    peers = [(partner(2 * d), tp) for d in range(1, PLANES)]
+    peers += [(partner(1), tp), (me, cross), (me, core)]
+    for peer in peers:
+        pl.semaphore_signal(barrier, inc=1, device_id=peer, device_id_type=MESH)
+
+    values = tokens[...].astype(f32)
+    scale = lax.rsqrt(jnp.mean(values * values, axis=-1, keepdims=True) + NORM_EPS)
+    for j in range(4):
+        for h in range(PARTS):
+            span = slice(j * quarter + h * width, j * quarter + (h + 1) * width)
+            normed[j, h] = (tokens[:, span].astype(f32) * scale * gain[:, span]).astype(bf16)
+    meta[0, 0:2] = ids[...].astype(f32)
+    meta[0, 2:4] = route[...]
+    pl.semaphore_wait(barrier, len(peers))
+    for d in range(1, PLANES):
+        describe(d).start()
+
+    def L(d, h):
+        for q in shares(d):
+            spread(d, q, h).start()
+
+    def M(d):
+        if d:
+            describe(d).wait_recv()
+        else:
+            earlier = lax.broadcasted_iota(jnp.int32, (tok_count, tok_count), 0)
+            later = lax.broadcasted_iota(jnp.int32, (tok_count, tok_count), 1)
+            before[...] = jnp.where(earlier < later, 1.0, 0.0).astype(bf16)
+        for side in range(2):
+            hits = meta[d, 0:2] == partner(side).astype(f32)
+            named = jnp.sum(jnp.where(hits, 1.0, 0.0), axis=0, keepdims=True)
+            weight = jnp.sum(jnp.where(hits, meta[d, 2:4], 0.0), axis=0, keepdims=True)
+            count = jnp.dot(
+                jnp.broadcast_to(named, (8, tok_count)).astype(bf16),
+                before[...],
+                preferred_element_type=f32,
+            )[0:1]
+            slot = jnp.where(named > 0.0, count.astype(jnp.int32), -1)
+            place = lax.broadcasted_iota(jnp.int32, (slots, tok_count), 0)
+            chosen = place == slot
+            mix = jnp.where(chosen, weight, 0.0)
+            mix_high = mix.astype(bf16)
+            high[d, side] = mix_high
+            low[d, side] = (mix - mix_high.astype(f32)).astype(bf16)
+            picker[d, side] = jnp.where(chosen, 1.0, 0.0).astype(bf16)
+
+    def block(d, q, h):
+        return dense[d - 1, q, h] if d else normed[quarters[q], h]
+
+    def pick(d, side, source):
+        return jnp.dot(picker[d, side], source, preferred_element_type=f32).astype(bf16)
+
+    arrived = set()
+
+    def arrive(d, h):
+        if d and (d, h) not in arrived:
+            arrived.add((d, h))
+            for q in shares(d):
+                spread(d, q, h).wait_recv()
+
+    def A(d, h):
+        if d == 0:
+            for j in range(4):
+                for n in range(PARTS):
+                    rows[0, j, n] = pick(0, 0, normed[j, n])
+            return
+        arrive(d, h)
+        for q in shares(d):
+            rows[2 * d, quarters[q], h] = pick(d, 0, block(d, q, h))
+            to_core(2 * d, q, h).start()
+        if len(shares(d)) == 1:
+            to_cross(2 * d, h).start()
+
+    def Y(d, h):
+        arrive(d, h)
+        for n in range(PARTS) if d == 0 else (h,):
+            for q in shares(d):
+                picked[d, q, n] = pick(d, 1, block(d, q, n))
+                neighbour(d, q, n).start()
+
+    def B(d, h):
+        k = 2 * d + 1
+        for q in shares(d):
+            neighbour(d, q, h).wait_recv()
+            to_core(k, q, h).start()
+        if len(shares(d)) == 1:
+            to_cross(k, h).start()
+
+    def X(d, side, h):
+        k = 2 * d + side
+        to_cross(k, h).wait_recv()
+        to_core(k, 1, h).start()
+
+    def F(d, side):
+        k = 2 * d + side
+        if (d, side) == FIRST:
+            for copy in weights:
+                copy.wait()
+        if k:
+            for q in range(2):
+                for h in range(PARTS):
+                    to_core(k, q, h).wait_recv()
+        whole = jnp.concatenate([rows[k, j, h] for j in range(4) for h in range(PARTS)], axis=1)
+        gate_sum = jnp.dot(whole, gate_w[...], preferred_element_type=f32)
+        up_sum = jnp.dot(whole, up_w[...], preferred_element_type=f32)
+        activated = activate(gate_sum, up_sum)
+        for j in range(4):
+            piece = jnp.dot(
+                activated, down_w[:, j * quarter : (j + 1) * quarter], preferred_element_type=f32
+            ).astype(bf16)
+            for h in range(PARTS):
+                part[k, j % 2, h, j // 2] = piece[:, h * width : (h + 1) * width]
+        for h in range(PARTS):
+            pair(k, h).start()
+
+    def G(d, side, h):
+        k = 2 * d + side
+        pair(k, h).wait_recv()
+        both = part[k, b, h, 1 - a].astype(f32) + pair_in[k, h, 1 - a].astype(f32)
+        cross_out[k, h] = both.astype(bf16)
+        cross_sum(k, h).start()
+
+    def H(d, side, h):
+        k = 2 * d + side
+        cross_sum(k, h).wait_recv()
+        both = part[k, b, h, a].astype(f32) + pair_in[k, h, a].astype(f32)
+        result[k, h] = (both + cross_in[k, h].astype(f32)).astype(bf16)
+        if side:
+            near_sum(d, h).start()
+
+    def S(d, h):
+        near_sum(d, h).wait_recv()
+        mixed = 0.0
+        for side, value in ((0, result[2 * d, h]), (1, plane_in[d, h])):
+            for share in (high, low):
+                mixed += lax.dot_general(
+                    share[d, side], value, (((0,), (0,)), ((), ())), preferred_element_type=f32
+                )
+        if d:
+            sum_out[d - 1, h] = mixed.astype(bf16)
+            plane_sum(d, h).start()
+        else:
+            total[h] = mixed
+
+    def J(d, h):
+        plane_sum(d, h).wait_recv()
+
+    stages = dict(L=L, M=M, A=A, Y=Y, B=B, X=X, F=F, G=G, H=H, S=S, J=J)
+    for step in STEPS:
+        stages[step[0]](*(int(n) for n in step[1:]))
+
+    for h in range(PARTS):
+        mixed = total[h]
+        for d in range(1, PLANES):
+            mixed += sum_in[d - 1, h].astype(f32)
+        out[:, h * width : (h + 1) * width] = mixed.astype(bf16)
+
+    for d in range(PLANES):
+        if d:
+            describe(d).wait_send()
+        for h in range(PARTS):
+            for q in shares(d):
+                neighbour(d, q, h).wait_send()
+                if d:
+                    spread(d, q, h).wait_send()
+            near_sum(d, h).wait_send()
+            if d:
+                plane_sum(d, h).wait_send()
+    for k in range(groups):
+        for h in range(PARTS):
+            pair(k, h).wait_send()
+            cross_sum(k, h).wait_send()
+            if k:
+                for q in range(2):
+                    to_core(k, q, h).wait_send()
+            if k >= PLANES:
+                to_cross(k, h).wait_send()
+
+
+FIRST = next((int(step[1]), int(step[2])) for step in STEPS if step[0] == "F")
+
+
+def plane_call(groups, capacity, operands):
+    tokens, weights = operands[0], operands[4:]
+    tok_count, model_width = tokens.shape
+    quarter = model_width // 4
+    width = quarter // PARTS
+    bf16, f32 = jnp.bfloat16, jnp.float32
+    compact = (PARTS, capacity, width)
+    full = (PARTS, tok_count, width)
+    dma = pltpu.SemaphoreType.DMA
+    return pl.pallas_call(
+        functools.partial(plane_kernel, groups),
+        out_shape=jax.ShapeDtypeStruct((tok_count, quarter), bf16),
+        in_specs=[pl.BlockSpec(memory_space=pltpu.VMEM)] * 4
+        + [pl.BlockSpec(memory_space=pl.ANY)] * 3,
+        out_specs=pl.BlockSpec(memory_space=pltpu.VMEM),
+        scratch_shapes=[
+            *[pltpu.VMEM(weight.shape, bf16) for weight in weights],
+            pltpu.VMEM((tok_count, tok_count), bf16),
+            pltpu.VMEM((PLANES, 8, tok_count), f32),
+            pltpu.VMEM((4, *full), bf16),
+            pltpu.VMEM((PLANES - 1, 2, *full), bf16),
+            *[pltpu.VMEM((PLANES, 2, capacity, tok_count), bf16)] * 3,
+            pltpu.VMEM((groups, 4, *compact), bf16),
+            pltpu.VMEM((PLANES, 2, *compact), bf16),
+            pltpu.VMEM((groups, 2, PARTS, 2, capacity, width), bf16),
+            pltpu.VMEM((groups, PARTS, 2, capacity, width), bf16),
+            *[pltpu.VMEM((groups, *compact), bf16)] * 3,
+            pltpu.VMEM((PLANES, *compact), bf16),
+            pltpu.VMEM(full, f32),
+            *[pltpu.VMEM((PLANES - 1, *full), bf16)] * 2,
+            dma((3,)),
+            *[dma((PLANES,))] * 2,
+            *[dma((PLANES, 2, PARTS))] * 4,
+            *[dma((groups, 2, PARTS))] * 2,
+            *[dma((groups, PARTS))] * 6,
+            *[dma((PLANES, PARTS))] * 4,
+        ],
+        compiler_params=pltpu.CompilerParams(
+            collective_id=0, has_side_effects=True, vmem_limit_bytes=60 * 1024 * 1024
+        ),
+    )(*operands)
 
 
 def expert_kernel(
@@ -319,6 +699,9 @@
     bf16 = jnp.bfloat16
     slots = (groups, capacity, quarter)
     weights = (expert_gate[0], expert_up[0], expert_down[0])
+    operands = (tokens, expert_ids.T, route_weight.T, norm_gain[None, :], *weights)
+    if groups == 2 * PLANES and 2 * capacity > tok_count:
+        return plane_call(groups, capacity, operands)
     return pl.pallas_call(
         functools.partial(expert_kernel, groups),
         out_shape=jax.ShapeDtypeStruct((tok_count, quarter), bf16),
@@ -348,7 +731,7 @@
         compiler_params=pltpu.CompilerParams(
             collective_id=0, has_side_effects=True, vmem_limit_bytes=60 * 1024 * 1024
         ),
-    )(tokens, expert_ids.T, route_weight.T, norm_gain[None, :], *weights)
+    )(*operands)
 
 
 def solution(mesh):

time: 87.9 us -> 84.9 us (0.966)
  Pallas kernels: 86 us -> 83 us
    pallas_call x1, Pallas kernels: 86 us -> 83 us  [plane_call(): pl.pallas_call(functools.partial(plane_kernel, groups), out_shape=jax.Sha...]
where the time goes in v2:
time: 84.9 us; the launch traced here: 84.7 us
  Pallas kernels  83 us (98%)
  local copies, waits for them, and re-layouts  1.67 us (2%)
    pallas_call x1, Pallas kernels, plane_call(): pl.pallas_call(functools.partial(plane_kernel, groups), out_shape=jax.Sha...  83 us

profile of v2, /device:TPU:0, one launch (start us, length us, event | category | flops | bytes accessed | tf_op | source)
XLA Modules:
  0.0 84.7 jit_solution(2438741539189808338)
XLA Ops:
  0.0 83.0 %shard_map.73 = bf16[256,512]{1,0:T(8,128)(2,1)} custom-call(bf16[256,2048]{1,0:T(8,128)(2,1)} %tokens.1, s32[2,256]{1,0:T(2,128)} %bitcast.10, f32[2,256]{1,0:T(2,128)} %bitcast.11, f32[1,2048]{1,0:T(1,128)} %bitcast.9, bf16[2048,512]{1,0:T(8,128)(2,1)} %bitcast.6, bf16[2048,512]{1,0:T(8,128)(2,1)} %bitcast.7, bf16[512,2048]{1,0:T(8,128)(2,1)} %bitcast.8), custom_call_target="tpu_custom_call" | custom-call | tf_op jit(solution)/shard_map/pallas_call | solution.py:368
  83.0 1.7 %copy.9 = bf16[256,512]{1,0:T(8,128)(2,1)} copy(bf16[256,512]{1,0:T(8,128)(2,1)} %shard_map.73) | data formatting | bytes 524288

commit v3 on v2

--- a/solution.py
+++ b/solution.py
@@ -12,19 +12,19 @@
 SWISH_SCALE = 1.702
 MESH = pl.DeviceIdType.MESH
 STEPS = (
-    "L30", "M0", "Y00", "A00", "L31", "F00", "G000", "G001", "L20", "M3",
-    "Y30", "A30", "L11", "B01", "L21", "H001", "B00", "B30", "A31", "F01",
-    "Y31", "G010", "X300", "M2", "A20", "Y20", "X301", "L10", "B31", "F30",
-    "B20", "Y21", "A21", "X310", "M1", "A11", "X311", "Y11", "G300", "F31",
-    "B21", "X210", "X200", "G311", "G310", "G301", "A10", "H300", "Y10", "X201",
-    "G011", "H000", "X211", "F10", "H311", "F20", "F21", "G100", "H301", "B11",
-    "H310", "B10", "G210", "S31", "G200", "F11", "H010", "S30", "G110", "G211",
-    "G111", "H210", "H200", "G201", "H011", "H100", "G101", "H110", "S20", "H211",
-    "J30", "H111", "S00", "S10", "H201", "H101", "S21", "J31", "J10", "S11",
-    "S01", "J20", "J11", "J21",
+    "L31", "L30", "L10", "M0", "Y00", "L21", "M3", "Y31", "B01", "B00",
+    "L11", "A31", "B31", "A30", "Y30", "F01", "M1", "Y10", "L20", "G010",
+    "B30", "X301", "M2", "Y21", "X311", "A21", "X300", "F30", "Y11", "G300",
+    "X310", "B10", "A11", "B21", "F31", "G311", "A10", "Y20", "H300", "G310",
+    "B11", "G301", "F10", "F11", "A20", "H311", "G100", "G110", "X211", "X201",
+    "G111", "H310", "B20", "F21", "H301", "S31", "G210", "H110", "G211", "S30",
+    "H010", "F20", "G200", "G101", "G201", "H210", "H100", "S10", "A00", "F00",
+    "H111", "H200", "S20", "J31", "G011", "H211", "G000", "J30", "H101", "S11",
+    "H201", "S21", "J10", "H011", "G001", "H001", "J20", "S01", "J11", "H000",
+    "S00", "J21",
 )
-PLANES = 1 + max(int(step[1]) for step in STEPS)
-PARTS = 2
+CARRIED = ((2, 2), (2, 2), (2, 1), (1, 1))
+PLANES, PARTS = len(CARRIED), len(CARRIED[0])
 
 
 def activate(gate_sum, up_sum):
@@ -46,6 +46,8 @@
     gate_w,
     up_w,
     down_w,
+    token_in,
+    out_part,
     before,
     meta,
     normed,
@@ -65,6 +67,7 @@
     sum_out,
     sum_in,
     w_sem,
+    io_sem,
     meta_send,
     meta_recv,
     dense_send,
@@ -94,6 +97,8 @@
     quarter = PARTS * width
     tok_count = tokens.shape[0]
     f32, bf16 = jnp.float32, jnp.bfloat16
+    fetch = pltpu.make_async_copy(tokens, token_in, io_sem.at[PARTS])
+    fetch.start()
 
     def partner(k):
         total, bit = 0, 1
@@ -112,8 +117,8 @@
             device_id_type=MESH,
         )
 
-    def shares(d):
-        return range(2 if d < PLANES // 2 else 1)
+    def shares(d, h):
+        return range(CARRIED[d][h])
 
     def describe(d):
         return remote(meta.at[0], meta.at[d], meta_send.at[d], meta_recv.at[d], 2 * d, tp)
@@ -170,21 +175,21 @@
         pltpu.make_async_copy(src, dst, w_sem.at[i])
         for i, (src, dst) in enumerate(((gate_hbm, gate_w), (up_hbm, up_w), (down_hbm, down_w)))
     ]
-    for copy in weights:
-        copy.start()
-
     barrier = pltpu.get_barrier_semaphore()
     peers = [(partner(2 * d), tp) for d in range(1, PLANES)]
     peers += [(partner(1), tp), (me, cross), (me, core)]
     for peer in peers:
         pl.semaphore_signal(barrier, inc=1, device_id=peer, device_id_type=MESH)
 
-    values = tokens[...].astype(f32)
+    fetch.wait()
+    for copy in weights:
+        copy.start()
+    values = token_in[...].astype(f32)
     scale = lax.rsqrt(jnp.mean(values * values, axis=-1, keepdims=True) + NORM_EPS)
     for j in range(4):
         for h in range(PARTS):
             span = slice(j * quarter + h * width, j * quarter + (h + 1) * width)
-            normed[j, h] = (tokens[:, span].astype(f32) * scale * gain[:, span]).astype(bf16)
+            normed[j, h] = (token_in[:, span].astype(f32) * scale * gain[:, span]).astype(bf16)
     meta[0, 0:2] = ids[...].astype(f32)
     meta[0, 2:4] = route[...]
     pl.semaphore_wait(barrier, len(peers))
@@ -192,7 +197,7 @@
         describe(d).start()
 
     def L(d, h):
-        for q in shares(d):
+        for q in shares(d, h):
             spread(d, q, h).start()
 
     def M(d):
@@ -231,7 +236,7 @@
     def arrive(d, h):
         if d and (d, h) not in arrived:
             arrived.add((d, h))
-            for q in shares(d):
+            for q in shares(d, h):
                 spread(d, q, h).wait_recv()
 
     def A(d, h):
@@ -241,25 +246,25 @@
                     rows[0, j, n] = pick(0, 0, normed[j, n])
             return
         arrive(d, h)
-        for q in shares(d):
+        for q in shares(d, h):
             rows[2 * d, quarters[q], h] = pick(d, 0, block(d, q, h))
             to_core(2 * d, q, h).start()
-        if len(shares(d)) == 1:
+        if len(shares(d, h)) == 1:
             to_cross(2 * d, h).start()
 
     def Y(d, h):
         arrive(d, h)
         for n in range(PARTS) if d == 0 else (h,):
-            for q in shares(d):
+            for q in shares(d, n):
                 picked[d, q, n] = pick(d, 1, block(d, q, n))
                 neighbour(d, q, n).start()
 
     def B(d, h):
         k = 2 * d + 1
-        for q in shares(d):
+        for q in shares(d, h):
             neighbour(d, q, h).wait_recv()
             to_core(k, q, h).start()
-        if len(shares(d)) == 1:
+        if len(shares(d, h)) == 1:
             to_cross(k, h).start()
 
     def X(d, side, h):
@@ -325,23 +330,30 @@
     for step in STEPS:
         stages[step[0]](*(int(n) for n in step[1:]))
 
+    def store(h):
+        span = pl.ds(h * width, width)
+        return pltpu.make_async_copy(out_part.at[h], out.at[:, span], io_sem.at[h])
+
     for h in range(PARTS):
         mixed = total[h]
         for d in range(1, PLANES):
             mixed += sum_in[d - 1, h].astype(f32)
-        out[:, h * width : (h + 1) * width] = mixed.astype(bf16)
+        out_part[h] = mixed.astype(bf16)
+        store(h).start()
 
     for d in range(PLANES):
         if d:
             describe(d).wait_send()
         for h in range(PARTS):
-            for q in shares(d):
+            for q in shares(d, h):
                 neighbour(d, q, h).wait_send()
                 if d:
                     spread(d, q, h).wait_send()
             near_sum(d, h).wait_send()
             if d:
                 plane_sum(d, h).wait_send()
+    for h in range(PARTS):
+        store(h).wait()
     for k in range(groups):
         for h in range(PARTS):
             pair(k, h).wait_send()
@@ -349,7 +361,7 @@
             if k:
                 for q in range(2):
                     to_core(k, q, h).wait_send()
-            if k >= PLANES:
+            if len(shares(k // 2, h)) == 1:
                 to_cross(k, h).wait_send()
 
 
@@ -368,11 +380,14 @@
     return pl.pallas_call(
         functools.partial(plane_kernel, groups),
         out_shape=jax.ShapeDtypeStruct((tok_count, quarter), bf16),
-        in_specs=[pl.BlockSpec(memory_space=pltpu.VMEM)] * 4
+        in_specs=[pl.BlockSpec(memory_space=pl.ANY)]
+        + [pl.BlockSpec(memory_space=pltpu.VMEM)] * 3
         + [pl.BlockSpec(memory_space=pl.ANY)] * 3,
-        out_specs=pl.BlockSpec(memory_space=pltpu.VMEM),
+        out_specs=pl.BlockSpec(memory_space=pl.ANY),
         scratch_shapes=[
             *[pltpu.VMEM(weight.shape, bf16) for weight in weights],
+            pltpu.VMEM(tokens.shape, bf16),
+            pltpu.VMEM(full, bf16),
             pltpu.VMEM((tok_count, tok_count), bf16),
             pltpu.VMEM((PLANES, 8, tok_count), f32),
             pltpu.VMEM((4, *full), bf16),
@@ -387,6 +402,7 @@
             pltpu.VMEM(full, f32),
             *[pltpu.VMEM((PLANES - 1, *full), bf16)] * 2,
             dma((3,)),
+            dma((PARTS + 1,)),
             *[dma((PLANES,))] * 2,
             *[dma((PLANES, 2, PARTS))] * 4,
             *[dma((groups, 2, PARTS))] * 2,

time: 84.9 us -> 77.1 us (0.908)
  Pallas kernels: 83 us -> 75.2 us
    pallas_call x1, Pallas kernels: 83 us -> 75.2 us  [plane_call(): pl.pallas_call(functools.partial(plane_kernel, groups), out_shape=jax.Sha...]
where the time goes in v3:
time: 77.1 us; the launch traced here: 76.9 us
  Pallas kernels  75.2 us (98%)
  local copies, waits for them, and re-layouts  1.67 us (2%)
    pallas_call x1, Pallas kernels, plane_call(): pl.pallas_call(functools.partial(plane_kernel, groups), out_shape=jax.Sha...  75.2 us
    unnamed x1, local copies, waits for them, and re-layouts  1.67 us

profile of v3, /device:TPU:0, one launch (start us, length us, event | category | flops | bytes accessed | tf_op | source)
XLA Modules:
  0.0 76.9 jit_solution(5330879113453209001)
XLA Ops:
  0.0 75.2 %shard_map.73 = bf16[256,512]{1,0:T(8,128)(2,1)} custom-call(bf16[256,2048]{1,0:T(8,128)(2,1)} %tokens.1, s32[2,256]{1,0:T(2,128)} %bitcast.10, f32[2,256]{1,0:T(2,128)} %bitcast.11, f32[1,2048]{1,0:T(1,128)} %bitcast.9, bf16[2048,512]{1,0:T(8,128)(2,1)} %bitcast.6, bf16[2048,512]{1,0:T(8,128)(2,1)} %bitcast.7, bf16[512,2048]{1,0:T(8,128)(2,1)} %bitcast.8), custom_call_target="tpu_custom_call" | custom-call | tf_op jit(solution)/shard_map/pallas_call | solution.py:380
  75.2 1.7 %copy.9 = bf16[256,512]{1,0:T(8,128)(2,1)} copy(bf16[256,512]{1,0:T(8,128)(2,1)} %shard_map.73) | data formatting | bytes 524288

commit v4 on v3

--- a/solution.py
+++ b/solution.py
@@ -47,7 +47,6 @@
     up_w,
     down_w,
     token_in,
-    out_part,
     before,
     meta,
     normed,
@@ -97,7 +96,7 @@
     quarter = PARTS * width
     tok_count = tokens.shape[0]
     f32, bf16 = jnp.float32, jnp.bfloat16
-    fetch = pltpu.make_async_copy(tokens, token_in, io_sem.at[PARTS])
+    fetch = pltpu.make_async_copy(tokens, token_in, io_sem)
     fetch.start()
 
     def partner(k):
@@ -120,15 +119,18 @@
     def shares(d, h):
         return range(CARRIED[d][h])
 
+    def settle(ref, sem):
+        pltpu.make_async_copy(ref, ref, sem).wait()
+
     def describe(d):
-        return remote(meta.at[0], meta.at[d], meta_send.at[d], meta_recv.at[d], 2 * d, tp)
+        return remote(meta.at[0], meta.at[d], meta_send, meta_recv.at[d], 2 * d, tp)
 
     def spread(d, q, h):
         return remote(
             normed.at[quarters[q], h],
             dense.at[d - 1, q, h],
-            dense_send.at[d, q, h],
-            dense_recv.at[d, q, h],
+            dense_send.at[d, h],
+            dense_recv.at[d, h],
             2 * d,
             tp,
         )
@@ -137,38 +139,38 @@
         return remote(
             picked.at[d, q, h],
             rows.at[2 * d + 1, quarters[q], h],
-            pick_send.at[d, q, h],
-            pick_recv.at[d, q, h],
+            pick_send.at[d, h],
+            pick_recv.at[d, h],
             1,
             tp,
         )
 
     def to_core(k, q, h):
         ref = rows.at[k, quarters[q], h]
-        return remote(ref, ref, core_send.at[k, q, h], core_recv.at[k, q, h], 0, core)
+        return remote(ref, ref, core_send, core_recv.at[k], 0, core)
 
     def to_cross(k, h):
         ref = rows.at[k, tp, h]
-        return remote(ref, ref, fwd_send.at[k, h], fwd_recv.at[k, h], 0, cross)
+        return remote(ref, ref, fwd_send, fwd_recv.at[k - PLANES, h], 0, cross)
 
     def pair(k, h):
         return remote(
-            part.at[k, 1 - b, h], pair_in.at[k, h], pair_send.at[k, h], pair_recv.at[k, h], 0, core
+            part.at[k, 1 - b, h], pair_in.at[k, h], pair_send, pair_recv.at[k, h], 0, core
         )
 
     def cross_sum(k, h):
         return remote(
-            cross_out.at[k, h], cross_in.at[k, h], cross_send.at[k, h], cross_recv.at[k, h], 0, cross
+            cross_out.at[k, h], cross_in.at[k, h], cross_send, cross_recv.at[k, h], 0, cross
         )
 
     def near_sum(d, h):
         return remote(
-            result.at[2 * d + 1, h], plane_in.at[d, h], near_send.at[d, h], near_recv.at[d, h], 1, tp
+            result.at[2 * d + 1, h], plane_in.at[d, h], near_send, near_recv.at[d, h], 1, tp
         )
 
     def plane_sum(d, h):
         return remote(
-            sum_out.at[d - 1, h], sum_in.at[d - 1, h], sum_send.at[d, h], sum_recv.at[d, h], 2 * d, tp
+            sum_out.at[d - 1, h], sum_in.at[d - 1, h], sum_send, sum_recv.at[d, h], 2 * d, tp
         )
 
     weights = [
@@ -236,8 +238,7 @@
     def arrive(d, h):
         if d and (d, h) not in arrived:
             arrived.add((d, h))
-            for q in shares(d, h):
-                spread(d, q, h).wait_recv()
+            settle(dense.at[d - 1, 0 : CARRIED[d][h], h], dense_recv.at[d, h])
 
     def A(d, h):
         if d == 0:
@@ -261,8 +262,8 @@
 
     def B(d, h):
         k = 2 * d + 1
+        settle(picked.at[d, 0 : CARRIED[d][h], h], pick_recv.at[d, h])
         for q in shares(d, h):
-            neighbour(d, q, h).wait_recv()
             to_core(k, q, h).start()
         if len(shares(d, h)) == 1:
             to_cross(k, h).start()
@@ -278,9 +279,7 @@
             for copy in weights:
                 copy.wait()
         if k:
-            for q in range(2):
-                for h in range(PARTS):
-                    to_core(k, q, h).wait_recv()
+            settle(rows.at[k, 0:2], core_recv.at[k])
         whole = jnp.concatenate([rows[k, j, h] for j in range(4) for h in range(PARTS)], axis=1)
         gate_sum = jnp.dot(whole, gate_w[...], preferred_element_type=f32)
         up_sum = jnp.dot(whole, up_w[...], preferred_element_type=f32)
@@ -330,39 +329,24 @@
     for step in STEPS:
         stages[step[0]](*(int(n) for n in step[1:]))
 
-    def store(h):
-        span = pl.ds(h * width, width)
-        return pltpu.make_async_copy(out_part.at[h], out.at[:, span], io_sem.at[h])
-
     for h in range(PARTS):
         mixed = total[h]
         for d in range(1, PLANES):
             mixed += sum_in[d - 1, h].astype(f32)
-        out_part[h] = mixed.astype(bf16)
-        store(h).start()
-
+        out[:, h * width : (h + 1) * width] = mixed.astype(bf16)
+
+    settle(meta.at[1:PLANES], meta_send)
     for d in range(PLANES):
-        if d:
-            describe(d).wait_send()
         for h in range(PARTS):
-            for q in shares(d, h):
-                neighbour(d, q, h).wait_send()
-                if d:
-                    spread(d, q, h).wait_send()
-            near_sum(d, h).wait_send()
+            settle(picked.at[d, 0 : CARRIED[d][h], h], pick_send.at[d, h])
             if d:
-                plane_sum(d, h).wait_send()
-    for h in range(PARTS):
-        store(h).wait()
-    for k in range(groups):
-        for h in range(PARTS):
-            pair(k, h).wait_send()
-            cross_sum(k, h).wait_send()
-            if k:
-                for q in range(2):
-                    to_core(k, q, h).wait_send()
-            if len(shares(k // 2, h)) == 1:
-                to_cross(k, h).wait_send()
+                settle(dense.at[d - 1, 0 : CARRIED[d][h], h], dense_send.at[d, h])
+    settle(rows.at[1:groups, 0:2], core_send)
+    settle(rows.at[0 : sum(carry.count(1) for carry in CARRIED) * 2 // PARTS, 0], fwd_send)
+    settle(part.at[:, 0], pair_send)
+    settle(cross_out, cross_send)
+    settle(plane_in, near_send)
+    settle(sum_out, sum_send)
 
 
 FIRST = next((int(step[1]), int(step[2])) for step in STEPS if step[0] == "F")
@@ -379,15 +363,14 @@
     dma = pltpu.SemaphoreType.DMA
     return pl.pallas_call(
         functools.partial(plane_kernel, groups),
-        out_shape=jax.ShapeDtypeStruct((tok_count, quarter), bf16),
+        out_shape=pltpu.VMEM((tok_count, quarter), bf16),
         in_specs=[pl.BlockSpec(memory_space=pl.ANY)]
         + [pl.BlockSpec(memory_space=pltpu.VMEM)] * 3
         + [pl.BlockSpec(memory_space=pl.ANY)] * 3,
-        out_specs=pl.BlockSpec(memory_space=pl.ANY),
+        out_specs=pl.BlockSpec(memory_space=pltpu.VMEM),
         scratch_shapes=[
             *[pltpu.VMEM(weight.shape, bf16) for weight in weights],
             pltpu.VMEM(tokens.shape, bf16),
-            pltpu.VMEM(full, bf16),
             pltpu.VMEM((tok_count, tok_count), bf16),
             pltpu.VMEM((PLANES, 8, tok_count), f32),
             pltpu.VMEM((4, *full), bf16),
@@ -402,12 +385,22 @@
             pltpu.VMEM(full, f32),
             *[pltpu.VMEM((PLANES - 1, *full), bf16)] * 2,
             dma((3,)),
-            dma((PARTS + 1,)),
-            *[dma((PLANES,))] * 2,
-            *[dma((PLANES, 2, PARTS))] * 4,
-            *[dma((groups, 2, PARTS))] * 2,
-            *[dma((groups, PARTS))] * 6,
+            dma,
+            dma,
+            dma((PLANES,)),
             *[dma((PLANES, PARTS))] * 4,
+            dma,
+            dma((groups,)),
+            dma,
+            dma((groups - PLANES, PARTS)),
+            dma,
+            dma((groups, PARTS)),
+            dma,
+            dma((groups, PARTS)),
+            dma,
+            dma((PLANES, PARTS)),
+            dma,
+            dma((PLANES, PARTS)),
         ],
         compiler_params=pltpu.CompilerParams(
             collective_id=0, has_side_effects=True, vmem_limit_bytes=60 * 1024 * 1024

time: 77.1 us -> 74 us (0.960)
  Pallas kernels: 75.2 us -> 73.1 us
  local copies, waits for them, and re-layouts: 1.67 us -> 0.71 us
    pallas_call x1, Pallas kernels: 75.2 us -> 73.1 us  [plane_call(): pl.pallas_call(functools.partial(plane_kernel, groups), out_shape=pltpu.V...]
    unnamed x1, local copies, waits for them, and re-layouts: 1.67 us -> 0.71 us
where the time goes in v4:
time: 74 us; the launch traced here: 73.8 us
  Pallas kernels  73.1 us (99%)
    pallas_call x1, Pallas kernels, plane_call(): pl.pallas_call(functools.partial(plane_kernel, groups), out_shape=pltpu.V...  73.1 us

profile of v4, /device:TPU:0, one launch (start us, length us, event | category | flops | bytes accessed | tf_op | source)
XLA Modules:
  0.0 73.8 jit_solution(17902241969772583881)
XLA Ops:
  0.0 73.1 %shard_map.73 = bf16[256,512]{1,0:T(8,128)(2,1)S(1)} custom-call(bf16[256,2048]{1,0:T(8,128)(2,1)} %tokens.1, s32[2,256]{1,0:T(2,128)} %bitcast.10, f32[2,256]{1,0:T(2,128)} %bitcast.11, f32[1,2048]{1,0:T(1,128)} %bitcast.9, bf16[2048,512]{1,0:T(8,128)(2,1)} %bitcast.6, bf16[2048,512]{1,0:T(8,128)(2,1)} %bitcast.7, bf16[512,2048]{1,0:T(8,128)(2,1)} %bitcast.8), custom_call_target="tpu_custom_call" | custom-call | tf_op jit(solution)/shard_map/pallas_call | solution.py:364
  73.1 0.7 copy.9

commit v5 on v4

--- a/solution.py
+++ b/solution.py
@@ -12,18 +12,26 @@
 SWISH_SCALE = 1.702
 MESH = pl.DeviceIdType.MESH
 STEPS = (
-    "L31", "L30", "L10", "M0", "Y00", "L21", "M3", "Y31", "B01", "B00",
-    "L11", "A31", "B31", "A30", "Y30", "F01", "M1", "Y10", "L20", "G010",
-    "B30", "X301", "M2", "Y21", "X311", "A21", "X300", "F30", "Y11", "G300",
-    "X310", "B10", "A11", "B21", "F31", "G311", "A10", "Y20", "H300", "G310",
-    "B11", "G301", "F10", "F11", "A20", "H311", "G100", "G110", "X211", "X201",
-    "G111", "H310", "B20", "F21", "H301", "S31", "G210", "H110", "G211", "S30",
-    "H010", "F20", "G200", "G101", "G201", "H210", "H100", "S10", "A00", "F00",
-    "H111", "H200", "S20", "J31", "G011", "H211", "G000", "J30", "H101", "S11",
-    "H201", "S21", "J10", "H011", "G001", "H001", "J20", "S01", "J11", "H000",
-    "S00", "J21",
+    "L13", "L33", "L32", "M0", "Y00", "A00", "F00", "G000", "G001", "B00",
+    "L11", "L30", "M3", "Y33", "G003", "L31", "A33", "Y32", "A32", "G002",
+    "M1", "A11", "B01", "L23", "L21", "L10", "B03", "A30", "Y30", "B33",
+    "A13", "B02", "X303", "Y31", "B32", "L22", "A31", "Y13", "X302", "F01",
+    "X300", "B30", "M2", "Y23", "B31", "A23", "G011", "G013", "H001", "Y11",
+    "X301", "L12", "F30", "G010", "X313", "L20", "Y21", "X310", "X311", "B13",
+    "X312", "A21", "B23", "H003", "A10", "Y10", "G300", "B11", "X203", "F31",
+    "B21", "Y22", "H000", "A12", "G310", "Y12", "A22", "G312", "F10", "G313",
+    "G311", "X211", "Y20", "H310", "B22", "B10", "H011", "B12", "G302", "H312",
+    "G301", "X201", "F11", "A20", "H010", "B20", "H300", "H311", "X213", "X202",
+    "G101", "X212", "H002", "G111", "G303", "S30", "F21", "H302", "G102", "G113",
+    "S32", "H313", "G210", "G112", "H101", "H301", "S31", "G211", "H111", "F20",
+    "G200", "G103", "H102", "G212", "H303", "H210", "G201", "G110", "G213", "S33",
+    "S11", "G202", "H112", "H211", "H113", "H200", "S20", "S00", "J32", "H013",
+    "G100", "G203", "S01", "H103", "S12", "H212", "H201", "S21", "H110", "J11",
+    "J30", "J33", "G012", "J31", "S13", "S03", "H213", "H202", "S22", "H100",
+    "S10", "J20", "H203", "S23", "J13", "H012", "J12", "S02", "J22", "J10",
+    "J21", "J23",
 )
-CARRIED = ((2, 2), (2, 2), (2, 1), (1, 1))
+CARRIED = ((2, 2, 2, 2), (2, 2, 2, 2), (2, 1, 1, 1), (1, 1, 1, 1))
 PLANES, PARTS = len(CARRIED), len(CARRIED[0])
 
 
@@ -47,6 +55,9 @@
     up_w,
     down_w,
     token_in,
+    id_in,
+    route_in,
+    gain_in,
     before,
     meta,
     normed,
@@ -96,8 +107,10 @@
     quarter = PARTS * width
     tok_count = tokens.shape[0]
     f32, bf16 = jnp.float32, jnp.bfloat16
-    fetch = pltpu.make_async_copy(tokens, token_in, io_sem)
-    fetch.start()
+    moves = ((tokens, token_in), (gain, gain_in), (ids, id_in), (route, route_in))
+    fetches = [pltpu.make_async_copy(*move, io_sem.at[i]) for i, move in enumerate(moves)]
+    for fetch in fetches:
+        fetch.start()
 
     def partner(k):
         total, bit = 0, 1
@@ -183,7 +196,8 @@
     for peer in peers:
         pl.semaphore_signal(barrier, inc=1, device_id=peer, device_id_type=MESH)
 
-    fetch.wait()
+    for fetch in fetches:
+        fetch.wait()
     for copy in weights:
         copy.start()
     values = token_in[...].astype(f32)
@@ -191,9 +205,9 @@
     for j in range(4):
         for h in range(PARTS):
             span = slice(j * quarter + h * width, j * quarter + (h + 1) * width)
-            normed[j, h] = (token_in[:, span].astype(f32) * scale * gain[:, span]).astype(bf16)
-    meta[0, 0:2] = ids[...].astype(f32)
-    meta[0, 2:4] = route[...]
+            normed[j, h] = (token_in[:, span].astype(f32) * scale * gain_in[:, span]).astype(bf16)
+    meta[0, 0:2] = id_in[...].astype(f32)
+    meta[0, 2:4] = route_in[...]
     pl.semaphore_wait(barrier, len(peers))
     for d in range(1, PLANES):
         describe(d).start()
@@ -342,7 +356,7 @@
             if d:
                 settle(dense.at[d - 1, 0 : CARRIED[d][h], h], dense_send.at[d, h])
     settle(rows.at[1:groups, 0:2], core_send)
-    settle(rows.at[0 : sum(carry.count(1) for carry in CARRIED) * 2 // PARTS, 0], fwd_send)
+    settle(rows.at[0 : sum(carry.count(1) for carry in CARRIED), 0, 0:2], fwd_send)
     settle(part.at[:, 0], pair_send)
     settle(cross_out, cross_send)
     settle(plane_in, near_send)
@@ -364,13 +378,11 @@
     return pl.pallas_call(
         functools.partial(plane_kernel, groups),
         out_shape=pltpu.VMEM((tok_count, quarter), bf16),
-        in_specs=[pl.BlockSpec(memory_space=pl.ANY)]
-        + [pl.BlockSpec(memory_space=pltpu.VMEM)] * 3
-        + [pl.BlockSpec(memory_space=pl.ANY)] * 3,
+        in_specs=[pl.BlockSpec(memory_space=pl.ANY)] * len(operands),
         out_specs=pl.BlockSpec(memory_space=pltpu.VMEM),
         scratch_shapes=[
             *[pltpu.VMEM(weight.shape, bf16) for weight in weights],
-            pltpu.VMEM(tokens.shape, bf16),
+            *[pltpu.VMEM(operands[n].shape, operands[n].dtype) for n in (0, 1, 2, 3)],
             pltpu.VMEM((tok_count, tok_count), bf16),
             pltpu.VMEM((PLANES, 8, tok_count), f32),
             pltpu.VMEM((4, *full), bf16),
@@ -385,7 +397,7 @@
             pltpu.VMEM(full, f32),
             *[pltpu.VMEM((PLANES - 1, *full), bf16)] * 2,
             dma((3,)),
-            dma,
+            dma((4,)),
             dma,
             dma((PLANES,)),
             *[dma((PLANES, PARTS))] * 4,

time: 74 us -> 70 us (0.946)
  Pallas kernels: 73.1 us -> 69.2 us
    pallas_call x1, Pallas kernels: 73.1 us -> 69.2 us  [plane_call(): pl.pallas_call(functools.partial(plane_kernel, groups), out_shape=pltpu.V...]
where the time goes in v5:
time: 70 us; the launch traced here: 69.9 us
  Pallas kernels  69.2 us (99%)
  local copies, waits for them, and re-layouts  0.71 us (1%)
    pallas_call x1, Pallas kernels, plane_call(): pl.pallas_call(functools.partial(plane_kernel, groups), out_shape=pltpu.V...  69.2 us

profile of v5, /device:TPU:0, one launch (start us, length us, event | category | flops | bytes accessed | tf_op | source)
XLA Modules:
  0.0 69.9 jit_solution(14275468183706381134)
XLA Ops:
  0.0 69.2 %shard_map.73 = bf16[256,512]{1,0:T(8,128)(2,1)S(1)} custom-call(bf16[256,2048]{1,0:T(8,128)(2,1)} %tokens.1, s32[2,256]{1,0:T(2,128)} %bitcast.10, f32[2,256]{1,0:T(2,128)} %bitcast.11, f32[1,2048]{1,0:T(1,128)} %bitcast.9, bf16[2048,512]{1,0:T(8,128)(2,1)} %bitcast.6, bf16[2048,512]{1,0:T(8,128)(2,1)} %bitcast.7, bf16[512,2048]{1,0:T(8,128)(2,1)} %bitcast.8), custom_call_target="tpu_custom_call" | custom-call | tf_op jit(solution)/shard_map/pallas_call | solution.py:378
  69.2 0.7 %copy.9 = bf16[256,512]{1,0:T(8,128)(2,1)} copy(bf16[256,512]{1,0:T(8,128)(2,1)S(1)} %shard_map.73) | data formatting | bytes 524288

commit v6 on v5

--- a/solution.py
+++ b/solution.py
@@ -12,13 +12,13 @@
 SWISH_SCALE = 1.702
 MESH = pl.DeviceIdType.MESH
 STEPS = (
-    "L13", "L33", "L32", "M0", "Y00", "A00", "F00", "G000", "G001", "B00",
+    "L13", "L33", "L32", "M0", "Y00", "A00", "F00", "G001", "B00", "G000",
     "L11", "L30", "M3", "Y33", "G003", "L31", "A33", "Y32", "A32", "G002",
     "M1", "A11", "B01", "L23", "L21", "L10", "B03", "A30", "Y30", "B33",
     "A13", "B02", "X303", "Y31", "B32", "L22", "A31", "Y13", "X302", "F01",
     "X300", "B30", "M2", "Y23", "B31", "A23", "G011", "G013", "H001", "Y11",
-    "X301", "L12", "F30", "G010", "X313", "L20", "Y21", "X310", "X311", "B13",
-    "X312", "A21", "B23", "H003", "A10", "Y10", "G300", "B11", "X203", "F31",
+    "X301", "L12", "F30", "G010", "X313", "L20", "Y21", "A21", "B13", "X310",
+    "X311", "X312", "H003", "A10", "B23", "Y10", "G300", "B11", "X203", "F31",
     "B21", "Y22", "H000", "A12", "G310", "Y12", "A22", "G312", "F10", "G313",
     "G311", "X211", "Y20", "H310", "B22", "B10", "H011", "B12", "G302", "H312",
     "G301", "X201", "F11", "A20", "H010", "B20", "H300", "H311", "X213", "X202",
@@ -26,8 +26,8 @@
     "S32", "H313", "G210", "G112", "H101", "H301", "S31", "G211", "H111", "F20",
     "G200", "G103", "H102", "G212", "H303", "H210", "G201", "G110", "G213", "S33",
     "S11", "G202", "H112", "H211", "H113", "H200", "S20", "S00", "J32", "H013",
-    "G100", "G203", "S01", "H103", "S12", "H212", "H201", "S21", "H110", "J11",
-    "J30", "J33", "G012", "J31", "S13", "S03", "H213", "H202", "S22", "H100",
+    "G100", "G203", "S01", "H103", "S12", "H212", "H201", "S21", "J30", "H110",
+    "J11", "J33", "G012", "J31", "S13", "S03", "H213", "H202", "S22", "H100",
     "S10", "J20", "H203", "S23", "J13", "H012", "J12", "S02", "J22", "J10",
     "J21", "J23",
 )

time: 70 us -> 70 us (level)
  no operation moved by 1% of the time
where the time goes in v6:
time: 70 us; the launch traced here: 69.8 us
  Pallas kernels  69.1 us (99%)
  local copies, waits for them, and re-layouts  0.71 us (1%)
    pallas_call x1, Pallas kernels, plane_call(): pl.pallas_call(functools.partial(plane_kernel, groups), out_shape=pltpu.V...  69.1 us

profile of v6, /device:TPU:0, one launch (start us, length us, event | category | flops | bytes accessed | tf_op | source)
XLA Modules:
  0.0 69.8 jit_solution(223098392161584933)
XLA Ops:
  0.0 69.1 %shard_map.73 = bf16[256,512]{1,0:T(8,128)(2,1)S(1)} custom-call(bf16[256,2048]{1,0:T(8,128)(2,1)} %tokens.1, s32[2,256]{1,0:T(2,128)} %bitcast.10, f32[2,256]{1,0:T(2,128)} %bitcast.11, f32[1,2048]{1,0:T(1,128)} %bitcast.9, bf16[2048,512]{1,0:T(8,128)(2,1)} %bitcast.6, bf16[2048,512]{1,0:T(8,128)(2,1)} %bitcast.7, bf16[512,2048]{1,0:T(8,128)(2,1)} %bitcast.8), custom_call_target="tpu_custom_call" | custom-call | tf_op jit(solution)/shard_map/pallas_call | solution.py:378
  69.1 0.7 %copy.9 = bf16[256,512]{1,0:T(8,128)(2,1)} copy(bf16[256,512]{1,0:T(8,128)(2,1)S(1)} %shard_map.73) | data formatting | bytes 524288
